TPU v7x, 256 devices: a whole 4x4x8 slice. The times are simulated.
256 devices in a mesh: ep: 64 (over z, y, core), tp: 4 (over x).
Axes of the slice: x: 4, y: 4, z: 8, core: 2. Of those that a mesh axis runs over, the one named last changes fastest.
Arguments:
- queries: bfloat16 [16384, 8, 128], P('ep', 'tp'), may hold values from -15 to 15
- keys: bfloat16 [16384, 4, 128], P('ep', 'tp'), may hold values from -6 to 6
- values: bfloat16 [16384, 4, 128], P('ep', 'tp'), may hold values from -6 to 6
- key_bias: bfloat16 [16384, 8], P('ep', 'tp'), may hold values from -20 to 2
- out_weight: bfloat16 [1024, 2048], P('tp'), may hold values from -0.1875 to 0.1875
- tokens_b: bfloat16 [32768, 2048], P(('ep', 'tp')), may hold values from -6 to 6
- moe_gain: bfloat16 [2048], replicated, may hold values from 0.099609375 to 1.8984375
- gate_weight: bfloat16 [64, 2048, 2048], P('ep', None, 'tp'), may hold values from -0.125 to 0.125
- up_weight: bfloat16 [64, 2048, 2048], P('ep', None, 'tp'), may hold values from -0.125 to 0.125
- down_weight: bfloat16 [64, 2048, 2048], P('ep', 'tp'), may hold values from -0.125 to 0.125
- routes: int32 [32768, 2], P(('ep', 'tp')), may hold values from 0 to 63, all different within a row; in each aligned block of 128 rows (0 to 127, 128 to 255, ...) at most 6 rows name the same one
- route_weights: float32 [32768, 2], P(('ep', 'tp')), may hold values from 0.2 to 1
Outputs:
- mixed: bfloat16 [16384, 2048], P(('ep', 'tp'))
- moe_out: bfloat16 [32768, 2048], P(('ep', 'tp'))
Inputs may be any that keep to these rules, and one draw needn't show every extreme that they name: `routes`: each row names 2 different experts. In each aligned block of 128 rows (the rows of one device) no expert is named by more than 6 rows, and in some block one expert is named by exactly 6 rows.
All inputs are finite; a program needn't handle non-finite values.
Results may differ from a plain program's by a relative error of at most 0.012.
Values may be sent and summed in bfloat16 or wider, within the bound.
A program may use at most 128 MiB of HBM per device.

v0:
```python
import math
import jax
import jax.numpy as jnp
from jax import lax
from jax.sharding import PartitionSpec as P


def in_one_piece(arrays, axis, dim, along):
    columns = [a.reshape(*a.shape[:along], -1) for a in arrays]
    both = jnp.concatenate(columns, axis=along)
    filled, at, done = (lax.all_gather(both, axis, axis=dim, tiled=True), 0, [])
    for a, column in zip(arrays, columns):
        share = filled[..., at : at + column.shape[along]]
        done.append(share.reshape(*share.shape[:along], *a.shape[along:]))
        at += column.shape[along]
    return tuple(done)


def partner(value, axis, apart):
    mask = 2**apart
    pairs = [(source, source ^ mask) for source in range(lax.axis_size(axis))]
    return lax.ppermute(value, axis, pairs)


def split_up(value, dim, length):
    before, after = (value.shape[:dim], value.shape[dim + 1 :])
    return jnp.moveaxis(value.reshape(*before, length, -1, *after), dim, 0)


def summed_on_arrival(value, axis, dim):
    pieces = split_up(value, dim, lax.axis_size(axis))
    arrived = lax.all_to_all(pieces, axis, split_axis=0, concat_axis=0, tiled=True)
    return arrived.astype(jnp.float32).sum(axis=0)


def entry_slots(routes, expert_total):
    flattened_expert_list = routes.reshape(-1)
    onehot = (
        flattened_expert_list[:, None] == jnp.arange(expert_total, dtype=jnp.int32)[None, :]
    ).astype(jnp.int32)
    earlier_count = jnp.cumsum(onehot, axis=0) - onehot
    return (flattened_expert_list, jnp.sum(earlier_count * onehot, axis=1))


def swiglu_rows(piece, gate_cols, up_cols):
    gate_val = jnp.dot(piece, gate_cols, preferred_element_type=jnp.float32)
    up_val = jnp.dot(piece, up_cols, preferred_element_type=jnp.float32)
    return (jax.nn.silu(gate_val) * up_val).astype(jnp.bfloat16)


def attend_rows(query_block, first_pos, keys_all, values_all, bias_all, local_kv):
    row_count, local_heads, head_dim = query_block.shape
    group_size = local_heads // local_kv
    key_total = keys_all.shape[0]
    key_span = min(1024, key_total)
    query_pos = first_pos + jnp.arange(row_count, dtype=jnp.int32)
    query_rows = query_block.reshape(row_count, local_kv, group_size, head_dim)
    visit_total = (first_pos + row_count + key_span - 1) // key_span
    score_scale = 1.0 / math.sqrt(head_dim)

    def visit(visit_no, state):
        accum, carried = state
        begin_at = (visit_total - 1 - visit_no) * key_span
        key_tile_rows = lax.dynamic_slice_in_dim(keys_all, begin_at, key_span, 0)
        value_block = lax.dynamic_slice_in_dim(values_all, begin_at, key_span, 0)
        bias_block = (
            lax.dynamic_slice_in_dim(bias_all, begin_at, key_span, 0)
            .astype(jnp.float32)
            .reshape(key_span, local_kv, group_size)
        )
        scores = (
            jnp.einsum(
                "rkgd,skd->kgrs", query_rows, key_tile_rows, preferred_element_type=jnp.float32
            )
            * score_scale
        )
        scores = scores + jnp.transpose(bias_block, (1, 2, 0))[:, :, None, :]
        key_pos = begin_at + jnp.arange(key_span, dtype=jnp.int32)
        earlier = key_pos[None, :] < query_pos[:, None]
        log_keep = jnp.where(earlier, jax.nn.log_sigmoid(-scores), 0.0)
        after = lax.cumsum(log_keep, axis=3, reverse=True) - log_keep
        weights = jnp.where(
            earlier, jnp.exp(jax.nn.log_sigmoid(scores) + after + carried[..., None]), 0.0
        ).astype(jnp.bfloat16)
        accum = accum + jnp.einsum(
            "kgrs,skd->kgrd", weights, value_block, preferred_element_type=jnp.float32
        )
        return (accum, carried + jnp.sum(log_keep, axis=3))

    start_state = (
        jnp.zeros((local_kv, group_size, row_count, head_dim), jnp.float32),
        jnp.zeros((local_kv, group_size, row_count), jnp.float32),
    )
    accum = lax.fori_loop(0, visit_total, visit, start_state)[0]
    return (
        jnp.transpose(accum, (2, 0, 1, 3))
        .reshape(row_count, local_heads * head_dim)
        .astype(jnp.bfloat16)
    )


def body(
    queries,
    keys,
    values,
    key_bias,
    out_weight,
    tokens_b,
    moe_gain,
    gate_weight,
    up_weight,
    down_weight,
    routes,
    route_weights,
):
    tok_rows, local_heads, head_dim = queries.shape
    local_kv = keys.shape[1]
    ep_count = lax.axis_size("ep")
    keys_all, values_all, bias_all = in_one_piece((keys, values, key_bias), "ep", 0, 1)
    device_ep = lax.axis_index("ep")
    half_rows = tok_rows // 2
    bit_count = ep_count.bit_length() - 1
    handed = queries[half_rows:]
    for bit_no in range(bit_count):
        handed = partner(handed, "ep", bit_no)
    companion_batch = ep_count - 1 - device_ep
    own_part = attend_rows(
        queries[:half_rows], device_ep * tok_rows, keys_all, values_all, bias_all, local_kv
    )
    other_part = attend_rows(
        handed, companion_batch * tok_rows + half_rows, keys_all, values_all, bias_all, local_kv
    )
    for bit_no in range(bit_count):
        other_part = partner(other_part, "ep", bit_no)
    attended = jnp.concatenate((own_part, other_part), axis=0)
    tok_b, model_width = tokens_b.shape
    top_count = routes.shape[1]
    expert_total = ep_count * gate_weight.shape[0]
    capacity = max(2, 3 * top_count * tok_b // (2 * expert_total))
    tokens_f = tokens_b.astype(jnp.float32)
    normed = (
        tokens_f
        * lax.rsqrt(jnp.mean(tokens_f * tokens_f, axis=1, keepdims=True) + 1e-06)
        * moe_gain.astype(jnp.float32)
    ).astype(jnp.bfloat16)
    flattened_expert_list, slot_index = entry_slots(routes, expert_total)
    place = flattened_expert_list * capacity + slot_index
    outbound = (
        jnp.zeros((expert_total * capacity, model_width), jnp.bfloat16)
        .at[place]
        .set(jnp.repeat(normed, top_count, axis=0))
    )
    outbound = outbound.reshape(expert_total, capacity, model_width)
    gate_cols = gate_weight[0]
    up_cols = up_weight[0]
    down_rows = down_weight[0]
    arrived = lax.all_to_all(outbound, "ep", split_axis=0, concat_axis=0, tiled=True)
    hidden = swiglu_rows(
        lax.all_gather(arrived.reshape(ep_count * capacity, model_width), "tp", axis=0, tiled=True),
        gate_cols,
        up_cols,
    )
    mixed_sum = lax.psum_scatter(
        jnp.dot(attended, out_weight, preferred_element_type=jnp.float32).astype(jnp.bfloat16),
        "tp",
        scatter_dimension=0,
        tiled=True,
    )
    expert_sum = summed_on_arrival(
        jnp.dot(hidden, down_rows, preferred_element_type=jnp.float32).astype(jnp.bfloat16), "tp", 0
    )
    returned = lax.all_to_all(
        expert_sum.astype(jnp.bfloat16).reshape(ep_count, capacity, model_width),
        "ep",
        split_axis=0,
        concat_axis=0,
        tiled=True,
    )
    picked = jnp.take(returned.reshape(expert_total * capacity, model_width), place, axis=0).astype(
        jnp.float32
    )
    weighted = picked * route_weights.reshape(-1)[:, None]
    moe_out = jnp.sum(weighted.reshape(tok_b, top_count, model_width), axis=1).astype(jnp.bfloat16)
    return (mixed_sum, moe_out)


def solution(mesh):
    in_specs = (
        P("ep", "tp", None),
        P("ep", "tp", None),
        P("ep", "tp", None),
        P("ep", "tp"),
        P("tp", None),
        P(("ep", "tp"), None),
        P(),
        P("ep", None, "tp"),
        P("ep", None, "tp"),
        P("ep", "tp", None),
        P(("ep", "tp"), None),
        P(("ep", "tp"), None),
    )
    out_specs = (P(("ep", "tp"), None), P(("ep", "tp"), None))
    return jax.shard_map(body, mesh=mesh, in_specs=in_specs, out_specs=out_specs, check_vma=False)
```

profile of v0, /device:TPU:8, one launch (start us, length us, event | category | flops | bytes accessed | tf_op | source)
XLA Modules:
  0.0 583.5 jit_solution(1064137814376958959)
XLA Ops:
  15.4 4.1 scatter_custom_fusion
  19.5 3.7 reshape.326
  23.2 63.4 %all_to_all.15 = bf16[64,6,2048]{2,1,0:T(8,128)(2,1)} all-to-all(bf16[64,6,2048]{2,1,0:T(8,128)(2,1)} %reshape.326), channel_id=1, replica_groups=mesh['ep'=64,'tp'=4] {'ep'}, dimensions={0} | all-to-all | bytes 3145728 | tf_op jit(solution)/shard_map/all_to_all | solution.py:157
  86.7 3.8 reshape.327
  93.4 3.7 collective-permute-done.1
  97.1 2.1 collective-permute-start.2
  99.2 3.7 collective-permute-done.2
  103.5 3.6 collective-permute-done.3
  107.3 5.1 collective-permute-done.4
  113.9 41.0 %all-gather.5.cloned.1.call-done = bf16[1536,2048]{1,0:T(8,128)(2,1)} async-done(((bf16[384,2048]{1,0:T(8,128)(2,1)}), bf16[1536,2048]{1,0:T(8,128)(2,1)}) %all-gather.5.cloned.1.call-update) | async-done | bytes 6291472 | tf_op jit(solution)/shard_map/all_gather | solution.py:159
  155.0 8.6 %fusion.53 = f32[1536,512]{1,0:T(8,128)} fusion(bf16[1536,2048]{1,0:T(8,128)(2,1)} %all-gather.5.cloned.1.call-done, bf16[1,2048,512]{2,1,0:T(8,128)(2,1)} %param.23), kind=kOutput, calls=%fused_computation.82 | convolution fusion | flops 3221225472 | bytes 11534336 | tf_op jit(solution)/shard_map/dot_general | solution.py:46
  163.6 11.8 %convolution_convert_fusion = bf16[1536,2048]{1,0:T(8,128)(2,1)} fusion(bf16[1,512,2048]{2,1,0:T(8,128)(2,1)S(1)} %copy-done, bf16[1536,2048]{1,0:T(8,128)(2,1)} %all-gather.5.cloned.1.call-done, f32[1536,512]{1,0:T(8,128)} %fusion.53, bf16[1,2048,512]{2,1,0:T(8,128)(2,1)} %param.24), kind=kOutput, calls=%fused_computation.74 | convolution fusion | flops 6450315264 | bytes 19922944 | tf_op jit(solution)/shard_map/dot_general | solution.py:170
  175.3 5.3 all-to-all-start.1
  180.6 66.6 %all-gather.3.cloned.1.call-done = bf16[16384,258]{1,0:T(8,128)(2,1)} async-done(((bf16[256,258]{1,0:T(8,128)(2,1)}), bf16[16384,258]{1,0:T(8,128)(2,1)}) %all-gather.3.cloned.1.call-update) | async-done | bytes 8454160 | tf_op jit(solution)/shard_map/all_gather | solution.py:11
  247.2 5.7 slice_bitcast_fusion.4
  252.9 3.8 slice.59
  256.7 3.7 copy.53
  260.5 125.5 %while.31 = (s32[]{:T(128)}, f32[1,2,128,128]{3,2,1,0:T(8,128)S(1)}, f32[1,2,128]{2,1,0:T(2,128)S(1)}, s32[]{:T(128)}, s32[]{:T(128)}, /*index=5*/bf16[16384,1,1...) while((s32[]{:T(128)}, ...), condition=%wide.region_9.10_spmd.clone, body=%wide.region_5.9_spmd.clone.sunk | while | flops 176343936 | bytes 10775775 | solution.py:94
  260.8 1.9 fusion.99
  262.7 2.5 fusion.100
  268.6 1.9 fusion.99
  270.5 2.5 fusion.100
  276.5 1.9 fusion.99
  278.4 2.5 fusion.100
  284.3 1.9 fusion.99
  286.2 2.5 fusion.100
  292.2 1.9 fusion.99
  294.1 2.5 fusion.100
  300.0 1.9 fusion.99
  301.9 2.5 fusion.100
  307.8 1.9 fusion.99
  309.7 2.5 fusion.100
  315.7 1.9 fusion.99
  317.6 2.5 fusion.100
  323.5 1.9 fusion.99
  325.4 2.5 fusion.100
  331.4 1.9 fusion.99
  333.3 2.5 fusion.100
  339.2 1.9 fusion.99
  341.1 2.5 fusion.100
  347.1 1.9 fusion.99
  349.0 2.5 fusion.100
  354.9 1.9 fusion.99
  356.8 2.5 fusion.100
  362.7 1.9 fusion.99
  364.6 2.5 fusion.100
  370.6 1.9 fusion.99
  372.5 2.5 fusion.100
  380.3 2.5 fusion.100
  387.5 2.0 collective-permute-start.7
  389.4 2.5 collective-permute-done.7
  391.9 5.8 collective-permute-done.8
  397.7 4.3 collective-permute-done.9
  402.0 5.3 collective-permute-done.10
  407.3 4.2 reduce_sum.69
  413.1 10.0 %all-to-all-start.2 = ((bf16[64,6,2048]{2,1,0:T(8,128)(2,1)}), bf16[64,6,2048]{2,1,0:T(8,128)(2,1)}, u32[]{:S(2)}, u32[]{:S(2)}) async-start(bf16[64,6,2048]{2,1,0:T(8,128)(2,1)} %reshape.329), calls=%async_computation.3 | async-start | bytes 4194304 | tf_op jit(solution)/shard_map/all_to_all | solution.py:172
  423.2 8.1 %while.30 = (s32[]{:T(128)}, f32[1,2,128,128]{3,2,1,0:T(8,128)S(1)}, f32[1,2,128]{2,1,0:T(2,128)S(1)}, s32[]{:T(128)}, s32[]{:T(128)}, /*index=5*/bf16[16384,1,1...) while((s32[]{:T(128)}, ...), condition=%wide.region_4.5_spmd.clone, body=%wide.region_0.4_spmd.clone.sunk | while | flops 176343936 | bytes 10775775 | solution.py:94
  425.4 2.5 fusion.93
  431.4 2.7 convolution_convert_fusion.1
  434.6 39.7 %all-to-all-done.2 = bf16[64,6,2048]{2,1,0:T(8,128)(2,1)} async-done(((bf16[64,6,2048]{2,1,0:T(8,128)(2,1)}), bf16[64,6,2048]{2,1,0:T(8,128)(2,1)}, u32[]{:S(2)}, u32[]{:S(2)}) %all-to-all-start.2) | async-done | bytes 1572896 | tf_op jit(solution)/shard_map/all_to_all | solution.py:172
  474.3 3.7 reshape.330
  478.0 4.1 gather_fusion
  483.6 6.2 %multiply_reduce_fusion = bf16[128,2048]{1,0:T(8,128)(2,1)} fusion(bf16[128,2,2048]{2,1,0:T(2,128)(2,1)} %gather.7, pred[128,2]{1,0:T(8,128)(4,1)S(1)} %copy.62, f32[128,2]{1,0:T(8,128)S(1)} %copy.64), kind=kLoop, calls=%fused_computation.84 | loop fusion | flops 1835008 | bytes 1574144 | tf_op jit(solution)/shard_map/reduce_sum | solution.py:183
  489.9 86.8 %reduce-scatter.2.cloned.1.call-done = bf16[64,2048]{1,0:T(8,128)(2,1)} async-done(((bf16[256,2048]{1,0:T(8,128)(2,1)}), bf16[64,2048]{1,0:T(8,128)(2,1)}) %reduce-scatter.2.cloned.1.call-update) | async-done | bytes 262160 | tf_op jit(solution)/shard_map/reduce_scatter | solution.py:163
  (264 shorter events, 78.7 us)
Async XLA Ops:
  7.2 156.4 %copy-start = (bf16[1,512,2048]{2,1,0:T(8,128)(2,1)S(1)}, bf16[1,512,2048]{2,1,0:T(8,128)(2,1)}, u32[]{:S(2)}) copy-start(bf16[1,512,2048]{2,1,0:T(8,128)(2,1)} %param.25) | copy-start | bytes 6291460
  7.2 147.8 %all-gather.5.cloned.1.call-start = ((), (), s32[]{:S(2)}) async-start(), calls=%async_computation.6 | async-start | bytes 7864320 | tf_op jit(solution)/shard_map/all_gather | solution.py:159
  86.6 3.8 copy-start.6
  86.7 4.0 copy-start.3
  86.7 4.0 copy-start.4
  86.7 4.7 copy-start.2
  90.4 156.8 %all-gather.3.cloned.1.call-start = ((), (), s32[]{:S(2)}) async-start(), calls=%async_computation.4 | async-start | bytes 12779520 | tf_op jit(solution)/shard_map/all_gather | solution.py:11
  91.5 1.3 collective-permute-start
  92.9 4.3 collective-permute-start.1
  97.1 5.8 collective-permute-start.2
  102.9 4.3 collective-permute-start.3
  107.2 5.2 collective-permute-start.4
  112.4 148.1 %collective-permute-start.5 = (bf16[128,2,128]{2,0,1:T(8,128)(2,1)S(1)}, bf16[128,2,128]{2,0,1:T(8,128)(2,1)S(1)}, u32[]{:S(2)}, u32[]{:S(2)}) collective-permute-start(bf16[128,2,128]{2,0,1:T(8,128)(2,1)S(1)} %collective-permute-done.4), channel_id=1, source_target_pairs={{0,128},{4,132},{8,136},{12,140},{16,144},{20,148},{24,152},{28,15... | collective-permute-start | bytes 196616 | tf_op jit(solution)/shard_map/ppermute | solution.py:22
  175.3 232.0 %all-to-all-start.1 = ((bf16[4,384,2048]{2,1,0:T(8,128)(2,1)}), bf16[4,384,2048]{2,1,0:T(8,128)(2,1)}, u32[]{:S(2)}, u32[]{:S(2)}) async-start(bf16[4,384,2048]{2,1,0:T(8,128)(2,1)} %bitcast.212), calls=%async_computation.2 | async-start | bytes 12582912 | tf_op jit(solution)/shard_map/all_to_all | solution.py:32
  386.1 1.3 collective-permute-start.6
  387.5 4.5 collective-permute-start.7
  391.9 5.8 collective-permute-start.8
  397.7 4.3 collective-permute-start.9
  402.0 5.3 collective-permute-start.10
  407.3 24.1 %collective-permute-start.11 = (bf16[128,256]{0,1:T(8,128)(2,1)S(1)}, bf16[128,256]{0,1:T(8,128)(2,1)S(1)}, u32[]{:S(2)}, u32[]{:S(2)}) collective-permute-start(bf16[128,256]{0,1:T(8,128)(2,1)S(1)} %collective-permute-done.10), channel_id=1, source_target_pairs={{0,128},{4,132},{8,136},{12,140},{16,144},{20,148},{24,152},{28,15... | collective-permute-start | bytes 196616 | tf_op jit(solution)/shard_map/ppermute | solution.py:22
  413.1 61.2 %all-to-all-start.2 = ((bf16[64,6,2048]{2,1,0:T(8,128)(2,1)}), bf16[64,6,2048]{2,1,0:T(8,128)(2,1)}, u32[]{:S(2)}, u32[]{:S(2)}) async-start(bf16[64,6,2048]{2,1,0:T(8,128)(2,1)} %reshape.329), calls=%async_computation.3 | async-start | bytes 4194304 | tf_op jit(solution)/shard_map/all_to_all | solution.py:172
  423.1 153.6 %reduce-scatter.2.cloned.1.call-start = ((), (), s32[]{:S(2)}) async-start(), calls=%async_computation.5 | async-start | bytes 1310720 | tf_op jit(solution)/shard_map/reduce_scatter | solution.py:163
  431.3 3.0 copy-start.5
  431.3 3.2 copy-start.7
  478.0 98.7 %copy-start.1 = (bf16[1,512,2048]{2,1,0:T(8,128)(2,1)S(1)}, bf16[1,512,2048]{2,1,0:T(8,128)(2,1)}, u32[]{:S(2)}) copy-start(bf16[1,512,2048]{2,1,0:T(8,128)(2,1)} %param.25) | copy-start | bytes 6291460
Sparse Core Ops, SparseCore 0:
  90.6 64.3 all-gather.4
  158.3 88.9 all-gather.2
  434.2 142.4 reduce-scatter.1
where the time goes:
time: 592 us; the launch traced here: 583 us
  waiting for transfers between devices  270 us (46%)
  other arithmetic  89.5 us (15%)
  matrix products  77.4 us (13%)
  blocking collectives  63.4 us (11%)
  local copies, waits for them, and re-layouts  43.9 us (7%)
  starting transfers between devices  22.8 us (4%)
  between operations  14.2 us (2%)
    reduce_scatter x1, waiting for transfers between devices, body(): lax.psum_scatter(jnp.dot(attended, out_weight, preferred_element_type=jnp...  86.8 us
    all_gather x1, waiting for transfers between devices, in_one_piece(): filled, at, done = (lax.all_gather(both, axis, axis=dim, tiled=True), 0, [])  66.6 us
    all_to_all x1, blocking collectives, body(): lax.all_to_all(outbound, 'ep', split_axis=0, concat_axis=0, tiled=True)  63.4 us
    another operation x36, other arithmetic  44.3 us
    all_gather x1, waiting for transfers between devices, body(): lax.all_gather(arrived.reshape(ep_count * capacity, model_width), 'tp', a...  41 us
    all_to_all x1, waiting for transfers between devices, body(): lax.all_to_all(expert_sum.astype(jnp.bfloat16).reshape(ep_count, capacity...  39.7 us
    ppermute x12, waiting for transfers between devices, partner(): return lax.ppermute(value, axis, pairs)  36.2 us
    dot_general x17, matrix products, visit(): jnp.einsum('rkgd,skd->kgrs', query_rows, key_tile_rows, preferred_element...  32.2 us
  transfers between devices with their start and end apart: 17, of which 14 were waited for; matrix products, arithmetic and copies ran while one was open for 33% of the time, Pallas kernels for 0%

commit v1 on v0

--- a/solution.py
+++ b/solution.py
@@ -155,8 +155,39 @@
     up_cols = up_weight[0]
     down_rows = down_weight[0]
     arrived = lax.all_to_all(outbound, "ep", split_axis=0, concat_axis=0, tiled=True)
+
+    def feed_levels_all_in(x_in, mesh_dim):
+        current_block, prior, side_arr = (
+            lax.axis_size(mesh_dim),
+            lax.axis_index(mesh_dim),
+            x_in.shape[0],
+        )
+        views = []
+        for dd in [*range(current_block)]:
+            views.append((dd, (dd + 1) % current_block))
+        vals = []
+        for dd in tuple(range(current_block)):
+            vals.append((dd, (dd - 1) % current_block))
+        view_out = jnp.zeros(
+            (*x_in.shape[:0], current_block * side_arr, *x_in.shape[1:]), x_in.dtype
+        )
+        view_out = lax.dynamic_update_slice_in_dim(view_out, x_in, prior * side_arr, axis=0)
+        seen_now = z1 = x_in
+        arr_next = current_block // 2
+        for c in tuple(range(1, arr_next + 1)):
+            seen_now = lax.ppermute(seen_now, mesh_dim, views)
+            view_out = lax.dynamic_update_slice_in_dim(
+                view_out, seen_now, (prior - c) % current_block * side_arr, axis=0
+            )
+            if c < current_block - arr_next:
+                z1 = lax.ppermute(z1, mesh_dim, vals)
+                view_out = lax.dynamic_update_slice_in_dim(
+                    view_out, z1, (prior + c) % current_block * side_arr, axis=0
+                )
+        return view_out
+
     hidden = swiglu_rows(
-        lax.all_gather(arrived.reshape(ep_count * capacity, model_width), "tp", axis=0, tiled=True),
+        feed_levels_all_in(arrived.reshape(ep_count * capacity, model_width), "tp"),
         gate_cols,
         up_cols,
     )

time: 592 us -> 548 us (0.926)
  waiting for transfers between devices: 270 us -> 203 us
  blocking collectives: 63.4 us -> 76.6 us
  local copies, waits for them, and re-layouts: 43.9 us -> 53.2 us
    all_gather x1, waiting for transfers between devices: 66.6 us -> 0.02 us  [in_one_piece(): filled, at, done = (lax.all_gather(both, axis, axis=dim, tiled=True), 0, [])]
    ppermute x0 -> x3, waiting for transfers between devices: none -> 43.5 us  [the longest x2 43.5 us: feed_levels_all_in(): seen_now = lax.ppermute(seen_now, mesh_dim, views)]
    all_gather x1 -> x0, waiting for transfers between devices: 41 us -> none  [body(): lax.all_gather(arrived.reshape(ep_count * capacity, model_width), 'tp', a...]
    all_to_all x1, waiting for transfers between devices: 39.7 us -> 0.01 us  [body(): lax.all_to_all(expert_sum.astype(jnp.bfloat16).reshape(ep_count, capacity...]
    ppermute x12, waiting for transfers between devices: 36.2 us -> 74.7 us  [partner(): return lax.ppermute(value, axis, pairs)]
    all_to_all x1, blocking collectives: 63.4 us -> 76.6 us  [body(): lax.all_to_all(outbound, 'ep', split_axis=0, concat_axis=0, tiled=True)]
  transfers between devices with their start and end apart: 17 -> 19, of which waited for: 14 -> 13; matrix products, arithmetic and copies ran while one was open for 33% -> 40% of each run, Pallas kernels for 0% -> 0%
where the time goes in v1:
time: 548 us; the launch traced here: 537 us
  waiting for transfers between devices  203 us (37%)
  other arithmetic  90.4 us (16%)
  blocking collectives  76.6 us (14%)
  matrix products  74.1 us (14%)
  local copies, waits for them, and re-layouts  53.2 us (10%)
  starting transfers between devices  23.8 us (4%)
  between operations  14.6 us (3%)
    reduce_scatter x1, waiting for transfers between devices, body(): lax.psum_scatter(jnp.dot(attended, out_weight, preferred_element_type=jnp...  84.5 us
    all_to_all x1, blocking collectives, body(): lax.all_to_all(outbound, 'ep', split_axis=0, concat_axis=0, tiled=True)  76.6 us
    ppermute x12, waiting for transfers between devices, partner(): return lax.ppermute(value, axis, pairs)  74.7 us
    another operation x36, other arithmetic  44.3 us
    ppermute x2, waiting for transfers between devices, feed_levels_all_in(): seen_now = lax.ppermute(seen_now, mesh_dim, views)  43.5 us
    dot_general x17, matrix products, visit(): jnp.einsum('rkgd,skd->kgrs', query_rows, key_tile_rows, preferred_element...  32.2 us
    convert_element_type x17, other arithmetic, visit(): weights = jnp.where(earlier, jnp.exp(jax.nn.log_sigmoid(scores) + after +...  26.1 us
    dot_general x17, matrix products, visit(): jnp.einsum('kgrs,skd->kgrd', weights, value_block, preferred_element_type...  22.1 us
  transfers between devices with their start and end apart: 19, of which 13 were waited for; matrix products, arithmetic and copies ran while one was open for 40% of the time, Pallas kernels for 0%

profile of v1, /device:TPU:8, one launch (start us, length us, event | category | flops | bytes accessed | tf_op | source)
XLA Modules:
  0.0 537.5 jit_solution(13042074682978981185)
XLA Ops:
  17.8 4.1 scatter_custom_fusion
  22.0 3.7 reshape.326
  25.7 76.6 %all_to_all.15 = bf16[64,6,2048]{2,1,0:T(8,128)(2,1)} all-to-all(bf16[64,6,2048]{2,1,0:T(8,128)(2,1)} %reshape.326), channel_id=1, replica_groups=mesh['ep'=64,'tp'=4] {'ep'}, dimensions={0} | all-to-all | bytes 3145728 | tf_op jit(solution)/shard_map/all_to_all | solution.py:157
  102.3 3.8 reshape.327
  109.3 34.0 %collective-permute-done.12 = bf16[384,2048]{1,0:T(8,128)(2,1)} collective-permute-done((bf16[384,2048]{1,0:T(8,128)(2,1)}, bf16[384,2048]{1,0:T(8,128)(2,1)}, u32[]{:S(2)}, u32[]{:S(2)}) %collective-permute-start.12) | collective-permute-done | bytes 1572896 | tf_op jit(solution)/shard_map/ppermute | solution.py:178
  144.8 4.3 collective-permute-done.1
  150.8 4.1 collective-permute-done.2
  154.9 4.3 collective-permute-done.3
  159.1 5.3 collective-permute-done.4
  170.2 9.5 %collective-permute-done.14 = bf16[384,2048]{1,0:T(8,128)(2,1)} collective-permute-done((bf16[384,2048]{1,0:T(8,128)(2,1)}, bf16[384,2048]{1,0:T(8,128)(2,1)}, u32[]{:S(2)}, u32[]{:S(2)}) %collective-permute-start.14) | collective-permute-done | bytes 1572896 | tf_op jit(solution)/shard_map/ppermute | solution.py:178
  181.3 2.6 copy-done.2
  183.9 5.3 fusion.55
  189.2 11.8 %convolution_convert_fusion = bf16[1536,2048]{1,0:T(8,128)(2,1)} fusion(bf16[1,512,2048]{2,1,0:T(8,128)(2,1)S(1)} %copy-done, f32[1536,512]{1,0:T(8,128)} %fusion.55, bf16[1536,2048]{1,0:T(8,128)(2,1)} %copy-done.2, bf16[1,2048,512]{2,1,0:T(8,128)(2,1)} %param.24), kind=kOutput, calls=%fused_computation.74 | convolution fusion | flops 6450315264 | bytes 19922944 | tf_op jit(solution)/shard_map/dot_general | solution.py:201
  201.1 5.2 all-to-all-start.1
  206.3 5.7 %slice_bitcast_fusion.4 = (bf16[16384,1,128]{2,0,1:T(8,128)(2,1)}, bf16[16384,1,128]{2,0,1:T(8,128)(2,1)}) fusion(bf16[16384,258]{1,0:T(8,128)(2,1)} %all-gather.2.cloned.1.call-done), kind=kLoop, calls=%fused_computation.75 | loop fusion | bytes 16777216 | tf_op jit(solution)/shard_map/reshape | solution.py:14
  212.0 3.8 slice.59
  215.8 3.7 copy.53
  219.6 125.7 %while.31 = (s32[]{:T(128)}, f32[1,2,128,128]{3,2,1,0:T(8,128)S(1)}, f32[1,2,128]{2,1,0:T(2,128)S(1)}, s32[]{:T(128)}, s32[]{:T(128)}, /*index=5*/bf16[16384,1,1...) while((s32[]{:T(128)}, ...), condition=%wide.region_9.10_spmd.clone, body=%wide.region_5.9_spmd.clone.sunk | while | flops 176343936 | bytes 10775783 | solution.py:94
  220.1 1.9 fusion.101
  222.0 2.5 fusion.102
  227.9 1.9 fusion.101
  229.8 2.5 fusion.102
  235.8 1.9 fusion.101
  237.6 2.5 fusion.102
  243.6 1.9 fusion.101
  245.5 2.5 fusion.102
  251.4 1.9 fusion.101
  253.3 2.5 fusion.102
  259.3 1.9 fusion.101
  261.2 2.5 fusion.102
  267.1 1.9 fusion.101
  269.0 2.5 fusion.102
  275.0 1.9 fusion.101
  276.9 2.5 fusion.102
  282.8 1.9 fusion.101
  284.7 2.5 fusion.102
  290.7 1.9 fusion.101
  292.6 2.5 fusion.102
  298.5 1.9 fusion.101
  300.4 2.5 fusion.102
  306.3 1.9 fusion.101
  308.2 2.5 fusion.102
  314.2 1.9 fusion.101
  316.1 2.5 fusion.102
  322.0 1.9 fusion.101
  323.9 2.5 fusion.102
  329.9 1.9 fusion.101
  331.8 2.5 fusion.102
  337.7 1.9 fusion.101
  339.6 2.5 fusion.102
  346.8 4.3 collective-permute-done.7
  351.0 5.8 %collective-permute-done.8 = bf16[128,256]{0,1:T(8,128)(2,1)S(1)} collective-permute-done((bf16[128,256]{0,1:T(8,128)(2,1)S(1)}, bf16[128,256]{0,1:T(8,128)(2,1)S(1)}, u32[]{:S(2)}, u32[]{:S(2)}) %collective-permute-start.8) | collective-permute-done | bytes 65568 | tf_op jit(solution)/shard_map/ppermute | solution.py:22
  356.8 4.3 collective-permute-done.9
  361.1 4.2 reduce_sum.69
  366.9 6.4 %all-to-all-start.2 = ((bf16[64,6,2048]{2,1,0:T(8,128)(2,1)}), bf16[64,6,2048]{2,1,0:T(8,128)(2,1)}, u32[]{:S(2)}, u32[]{:S(2)}) async-start(bf16[64,6,2048]{2,1,0:T(8,128)(2,1)} %reshape.329), calls=%async_computation.3 | async-start | bytes 4194304 | tf_op jit(solution)/shard_map/all_to_all | solution.py:203
  373.3 5.6 %collective-permute-start.11 = (bf16[128,256]{0,1:T(8,128)(2,1)S(1)}, bf16[128,256]{0,1:T(8,128)(2,1)S(1)}, u32[]{:S(2)}, u32[]{:S(2)}) collective-permute-start(bf16[128,256]{0,1:T(8,128)(2,1)S(1)} %collective-permute-done.10), channel_id=1, source_target_pairs={{0,128},{4,132},{8,136},{12,140},{16,144},{20,148},{24,152},{28,15... | collective-permute-start | bytes 196616 | tf_op jit(solution)/shard_map/ppermute | solution.py:22
  378.9 8.1 %while.30 = (s32[]{:T(128)}, f32[1,2,128,128]{3,2,1,0:T(8,128)S(1)}, f32[1,2,128]{2,1,0:T(2,128)S(1)}, s32[]{:T(128)}, s32[]{:T(128)}, /*index=5*/bf16[16384,1,1...) while((s32[]{:T(128)}, ...), condition=%wide.region_4.5_spmd.clone, body=%wide.region_0.4_spmd.clone.sunk | while | flops 176343936 | bytes 10775783 | solution.py:94
  381.3 2.5 fusion.95
  387.1 40.0 %collective-permute-done.11 = bf16[128,256]{0,1:T(8,128)(2,1)S(1)} collective-permute-done((bf16[128,256]{0,1:T(8,128)(2,1)S(1)}, bf16[128,256]{0,1:T(8,128)(2,1)S(1)}, u32[]{:S(2)}, u32[]{:S(2)}) %collective-permute-start.11) | collective-permute-done | bytes 65568 | tf_op jit(solution)/shard_map/ppermute | solution.py:22
  427.1 2.7 convolution_convert_fusion.1
  430.3 3.7 reshape.330
  434.1 4.1 gather_fusion
  439.7 6.2 %multiply_reduce_fusion = bf16[128,2048]{1,0:T(8,128)(2,1)} fusion(bf16[128,2,2048]{2,1,0:T(2,128)(2,1)} %gather.7, pred[128,2]{1,0:T(8,128)(4,1)S(1)} %copy.62, f32[128,2]{1,0:T(8,128)S(1)} %copy.64), kind=kLoop, calls=%fused_computation.84 | loop fusion | flops 1835008 | bytes 1574144 | tf_op jit(solution)/shard_map/reduce_sum | solution.py:214
  445.9 84.5 %reduce-scatter.2.cloned.1.call-done = bf16[64,2048]{1,0:T(8,128)(2,1)} async-done(((bf16[256,2048]{1,0:T(8,128)(2,1)}), bf16[64,2048]{1,0:T(8,128)(2,1)}) %reduce-scatter.2.cloned.1.call-update) | async-done | bytes 262160 | tf_op jit(solution)/shard_map/reduce_scatter | solution.py:194
  (272 shorter events, 87.8 us)
Async XLA Ops:
  7.2 182.1 %copy-start = (bf16[1,512,2048]{2,1,0:T(8,128)(2,1)S(1)}, bf16[1,512,2048]{2,1,0:T(8,128)(2,1)}, u32[]{:S(2)}) copy-start(bf16[1,512,2048]{2,1,0:T(8,128)(2,1)} %param.25) | copy-start | bytes 6291460
  7.2 199.2 %all-gather.2.cloned.1.call-start = ((), (), s32[]{:S(2)}) async-start(), calls=%async_computation.4 | async-start | bytes 12779520 | tf_op jit(solution)/shard_map/all_gather | solution.py:11
  25.7 117.7 %copy-start.4 = (bf16[256,2,128]{2,1,0:T(2,128)(2,1)S(1)}, bf16[256,2,128]{2,1,0:T(2,128)(2,1)}, u32[]{:S(2)}) copy-start(bf16[256,2,128]{2,1,0:T(2,128)(2,1)} %param.16) | copy-start | bytes 393220
  106.1 37.2 %collective-permute-start.12 = (bf16[384,2048]{1,0:T(8,128)(2,1)}, bf16[384,2048]{1,0:T(8,128)(2,1)}, u32[]{:S(2)}, u32[]{:S(2)}) collective-permute-start(bf16[384,2048]{1,0:T(8,128)(2,1)} %reshape.327), channel_id=1, source_target_pairs={{0,1},{1,2},{2,3},{3,0},{4,5},{5,6},{6,7},{7,4},{8,9},{9,10},{10,1... | collective-permute-start | bytes 4718600 | tf_op jit(solution)/shard_map/ppermute | solution.py:178
  107.6 60.9 %collective-permute-start.13 = (bf16[384,2048]{1,0:T(8,128)(2,1)}, bf16[384,2048]{1,0:T(8,128)(2,1)}, u32[]{:S(2)}, u32[]{:S(2)}) collective-permute-start(bf16[384,2048]{1,0:T(8,128)(2,1)} %reshape.327), channel_id=1, source_target_pairs={{0,3},{1,0},{2,1},{3,2},{4,7},{5,4},{6,5},{7,6},{8,11},{9,8},{10,9... | collective-permute-start | bytes 4718600 | tf_op jit(solution)/shard_map/ppermute | solution.py:183
  143.3 36.4 %collective-permute-start.14 = (bf16[384,2048]{1,0:T(8,128)(2,1)}, bf16[384,2048]{1,0:T(8,128)(2,1)}, u32[]{:S(2)}, u32[]{:S(2)}) collective-permute-start(bf16[384,2048]{1,0:T(8,128)(2,1)} %collective-permute-done.12), channel_id=1, source_target_pairs={{0,1},{1,2},{2,3},{3,0},{4,5},{5,6},{6,7},{7,4},{8,9},{9,10},{10,1... | collective-permute-start | bytes 4718600 | tf_op jit(solution)/shard_map/ppermute | solution.py:178
  143.5 1.3 collective-permute-start
  144.8 4.3 collective-permute-start.1
  149.1 5.8 %collective-permute-start.2 = (bf16[128,2,128]{2,0,1:T(8,128)(2,1)S(1)}, bf16[128,2,128]{2,0,1:T(8,128)(2,1)S(1)}, u32[]{:S(2)}, u32[]{:S(2)}) collective-permute-start(bf16[128,2,128]{2,0,1:T(8,128)(2,1)S(1)} %collective-permute-done.1), channel_id=1, source_target_pairs={{0,16},{4,20},{8,24},{12,28},{16,0},{20,4},{24,8},{28,12},{32,48},... | collective-permute-start | bytes 196616 | tf_op jit(solution)/shard_map/ppermute | solution.py:22
  154.9 4.3 collective-permute-start.3
  159.1 5.3 collective-permute-start.4
  159.1 7.5 %copy-start.3 = (bf16[384,2048]{1,0:T(8,128)(2,1)S(1)}, bf16[384,2048]{1,0:T(8,128)(2,1)}, u32[]{:S(2)}) copy-start(bf16[384,2048]{1,0:T(8,128)(2,1)} %reshape.327) | copy-start | bytes 4718596
  164.4 55.1 %collective-permute-start.5 = (bf16[128,2,128]{2,0,1:T(8,128)(2,1)S(1)}, bf16[128,2,128]{2,0,1:T(8,128)(2,1)S(1)}, u32[]{:S(2)}, u32[]{:S(2)}) collective-permute-start(bf16[128,2,128]{2,0,1:T(8,128)(2,1)S(1)} %collective-permute-done.4), channel_id=1, source_target_pairs={{0,128},{4,132},{8,136},{12,140},{16,144},{20,148},{24,152},{28,15... | collective-permute-start | bytes 196616 | tf_op jit(solution)/shard_map/ppermute | solution.py:22
  168.4 15.5 %copy-start.7 = (bf16[1,2048,512]{2,1,0:T(8,128)(2,1)S(1)}, bf16[1,2048,512]{2,1,0:T(8,128)(2,1)}, u32[]{:S(2)}) copy-start(bf16[1,2048,512]{2,1,0:T(8,128)(2,1)} %param.23) | copy-start | bytes 6291460
  181.3 2.6 copy-start.2
  201.1 160.0 %all-to-all-start.1 = ((bf16[4,384,2048]{2,1,0:T(8,128)(2,1)}), bf16[4,384,2048]{2,1,0:T(8,128)(2,1)}, u32[]{:S(2)}, u32[]{:S(2)}) async-start(bf16[4,384,2048]{2,1,0:T(8,128)(2,1)} %bitcast.214), calls=%async_computation.2 | async-start | bytes 12582912 | tf_op jit(solution)/shard_map/all_to_all | solution.py:32
  345.4 1.3 collective-permute-start.6
  346.8 4.3 collective-permute-start.7
  351.0 5.8 %collective-permute-start.8 = (bf16[128,256]{0,1:T(8,128)(2,1)S(1)}, bf16[128,256]{0,1:T(8,128)(2,1)S(1)}, u32[]{:S(2)}, u32[]{:S(2)}) collective-permute-start(bf16[128,256]{0,1:T(8,128)(2,1)S(1)} %collective-permute-done.7), channel_id=1, source_target_pairs={{0,16},{4,20},{8,24},{12,28},{16,0},{20,4},{24,8},{28,12},{32,48},... | collective-permute-start | bytes 196616 | tf_op jit(solution)/shard_map/ppermute | solution.py:22
  356.8 4.3 collective-permute-start.9
  361.1 12.3 %collective-permute-start.10 = (bf16[128,256]{0,1:T(8,128)(2,1)S(1)}, bf16[128,256]{0,1:T(8,128)(2,1)S(1)}, u32[]{:S(2)}, u32[]{:S(2)}) collective-permute-start(bf16[128,256]{0,1:T(8,128)(2,1)S(1)} %collective-permute-done.9), channel_id=1, source_target_pairs={{0,64},{4,68},{8,72},{12,76},{16,80},{20,84},{24,88},{28,92},{32,9... | collective-permute-start | bytes 196616 | tf_op jit(solution)/shard_map/ppermute | solution.py:22
  366.9 63.5 %all-to-all-start.2 = ((bf16[64,6,2048]{2,1,0:T(8,128)(2,1)}), bf16[64,6,2048]{2,1,0:T(8,128)(2,1)}, u32[]{:S(2)}, u32[]{:S(2)}) async-start(bf16[64,6,2048]{2,1,0:T(8,128)(2,1)} %reshape.329), calls=%async_computation.3 | async-start | bytes 4194304 | tf_op jit(solution)/shard_map/all_to_all | solution.py:203
  373.3 157.1 %reduce-scatter.2.cloned.1.call-start = ((), (), s32[]{:S(2)}) async-start(), calls=%async_computation.5 | async-start | bytes 1310720 | tf_op jit(solution)/shard_map/reduce_scatter | solution.py:194
  373.3 53.8 %collective-permute-start.11 = (bf16[128,256]{0,1:T(8,128)(2,1)S(1)}, bf16[128,256]{0,1:T(8,128)(2,1)S(1)}, u32[]{:S(2)}, u32[]{:S(2)}) collective-permute-start(bf16[128,256]{0,1:T(8,128)(2,1)S(1)} %collective-permute-done.10), channel_id=1, source_target_pairs={{0,128},{4,132},{8,136},{12,140},{16,144},{20,148},{24,152},{28,15... | collective-permute-start | bytes 196616 | tf_op jit(solution)/shard_map/ppermute | solution.py:22
  387.0 43.0 %copy-start.5 = (s32[128,2]{0,1:T(2,128)S(1)}, s32[128,2]{0,1:T(2,128)}, u32[]{:S(2)}) copy-start(s32[128,2]{0,1:T(2,128)} %param.26) | copy-start | bytes 3076
  387.0 43.2 %copy-start.6 = (f32[128,2]{0,1:T(2,128)S(1)}, f32[128,2]{0,1:T(2,128)}, u32[]{:S(2)}) copy-start(f32[128,2]{0,1:T(2,128)} %param.27) | copy-start | bytes 3076
  434.1 96.4 %copy-start.1 = (bf16[1,512,2048]{2,1,0:T(8,128)(2,1)S(1)}, bf16[1,512,2048]{2,1,0:T(8,128)(2,1)}, u32[]{:S(2)}) copy-start(bf16[1,512,2048]{2,1,0:T(8,128)(2,1)} %param.25) | copy-start | bytes 6291460
Sparse Core Ops, SparseCore 0:
  11.3 110.3 all-gather.1
  429.9 100.4 reduce-scatter.1
